TPU v7x, 32 devices: a whole 2x2x4 slice. The times are simulated.
32 devices in a mesh: fs: 8 (over z, y), tp: 4 (over x, core).
Axes of the slice: x: 2, y: 2, z: 4, core: 2. Of those that a mesh axis runs over, the one named last changes fastest.
Arguments:
- tokens: bfloat16 [6144, 2048], P('fs', 'tp'), may hold values from -40 to 40
- gain_one: float32 [2048], P('tp'), may hold values from 0.1 to 1.9
- w_gate: float32 [2048, 3072], P('fs', 'tp'), may hold values from -0.125 to 0.125
- w_up: float32 [2048, 3072], P('fs', 'tp'), may hold values from -0.125 to 0.125
- w_down: float32 [3072, 2048], P('tp', 'fs'), may hold values from -0.109375 to 0.109375
- scale_gate: float32 [3072], P('tp'), may hold values from 0.5 to 2
- scale_up: float32 [3072], P('tp'), may hold values from 0.5 to 2
- scale_down: float32 [2048], P('tp'), may hold values from 0.5 to 2
- gain_mix: float32 [2048], P('tp'), may hold values from 0.1 to 1.9
- w_query: float32 [2048, 2048], P('fs', 'tp'), may hold values from -0.125 to 0.125
- w_key: float32 [2048, 2048], P('fs', 'tp'), may hold values from -0.125 to 0.125
- w_value: float32 [2048, 2048], P('fs', 'tp'), may hold values from -0.125 to 0.125
- w_outgate: float32 [2048, 2048], P('fs', 'tp'), may hold values from -0.125 to 0.125
- scale_query: float32 [2048], P('tp'), may hold values from 0.5 to 2
- scale_key: float32 [2048], P('tp'), may hold values from 0.5 to 2
- scale_value: float32 [2048], P('tp'), may hold values from 0.5 to 2
- scale_outgate: float32 [2048], P('tp'), may hold values from 0.5 to 2
- ret_gain: float32 [2048], P('tp'), may hold values from 0.1 to 1.9
- decay_rate: float32 [8], P('tp'), may hold values from 0 to 2
- w_mix: float32 [2048, 2048], P('tp', 'fs'), may hold values from -0.125 to 0.125
- scale_mix: float32 [2048], P('tp'), may hold values from 0.5 to 2
- gain_two: float32 [2048], P('tp'), may hold values from 0.1 to 1.9
Outputs:
- layer_out: bfloat16 [6144, 2048], P('fs', 'tp')
All inputs are finite; a program needn't handle non-finite values.
Results may differ from a plain program's by a relative error of at most 0.022.
Values may be sent and summed in bfloat16 or wider, within the bound.
A program may use at most 128 MiB of HBM per device.

v0:
```python
import functools

import jax
import jax.numpy as jnp
import numpy as np
from jax import lax
from jax.experimental import pallas as pl
from jax.experimental.pallas import tpu as pltpu
from jax.sharding import PartitionSpec as P

LEN = 256
EPS = 1e-06
HEAD_EPS = 0.1
MESH = pl.DeviceIdType.MESH
BF16 = jnp.bfloat16
F32 = jnp.float32


def rows_of(ref, piece, rows):
    return ref.at[pl.ds(piece * rows, rows)]


def cols_at(index, width):
    return pl.ds(pl.multiple_of(index * width, width), width)


def remote(src, dst, send_sem, recv_sem, axis, target):
    return pltpu.make_async_remote_copy(
        src_ref=src,
        dst_ref=dst,
        send_sem=send_sem,
        recv_sem=recv_sem,
        device_id={axis: target},
        device_id_type=MESH,
    )


class TpGather:
    def __init__(self, ntp, src, out, sends, forwards, recvs, pieces):
        self.t = lax.axis_index("tp")
        self.nx = ntp // 2
        self.core = lax.rem(self.t, 2)
        self.chip = lax.div(self.t, 2)
        self.partner = self.chip * 2 + (1 - self.core)
        self.src, self.out = src, out
        self.sends, self.forwards, self.recvs = sends, forwards, recvs
        self.pieces = pieces
        self.rows = src.shape[0] // pieces
        self.width = src.shape[1]

    def along_x(self, offset, core):
        return lax.rem(self.chip + offset, self.nx) * 2 + core

    def place(self, index, piece):
        return self.out.at[pl.ds(piece * self.rows, self.rows), cols_at(index, self.width)]

    def own_sends(self, piece):
        src = rows_of(self.src, piece, self.rows)
        copies = []
        for offset in range(self.nx - 1, -1, -1):
            target = self.along_x(offset, self.core) if offset else self.partner
            copies.append(
                remote(
                    src,
                    self.place(self.t, piece),
                    self.sends.at[offset, piece],
                    self.recvs.at[self.t, piece],
                    "tp",
                    target,
                )
            )
        return copies

    def forward(self, offset, piece):
        index = self.along_x(self.nx - offset, self.core)
        block = self.place(index, piece)
        return remote(
            block,
            block,
            self.forwards.at[offset, piece],
            self.recvs.at[index, piece],
            "tp",
            self.partner,
        )

    def arrived(self, index, piece):
        block = self.place(index, piece)
        remote(
            block,
            block,
            self.sends.at[0, piece],
            self.recvs.at[index, piece],
            "tp",
            self.partner,
        ).wait_recv()

    def start(self, piece):
        for copy in self.own_sends(piece):
            copy.start()

    def relay(self):
        for piece in range(self.pieces):
            for offset in range(1, self.nx):
                self.arrived(self.along_x(self.nx - offset, self.core), piece)
                self.forward(offset, piece).start()

    def finish(self):
        for piece in range(self.pieces):
            for offset in range(self.nx):
                self.arrived(self.along_x(offset, 1 - self.core), piece)
        for piece in range(self.pieces):
            for copy in self.own_sends(piece):
                copy.wait_send()
            for offset in range(1, self.nx):
                self.forward(offset, piece).wait_send()


class FsGather:
    def __init__(self, nfs, ny, pieces, sends, recvs):
        self.ny, self.nz = ny, nfs // ny
        self.f = lax.axis_index("fs")
        self.z, self.y = lax.div(self.f, ny), lax.rem(self.f, ny)
        self.pieces = pieces
        self.sends, self.recvs = sends, recvs

    def source(self, p):
        src, _, _, part, parts, _ = self.pieces[p]
        step = src.shape[0] // parts
        return src.at[pl.ds(part * step, step)]

    def place(self, p, index):
        src, out, dim, part, parts, _ = self.pieces[p]
        rows, cols = src.shape
        step = rows // parts
        if dim == 0:
            return out.at[pl.ds(pl.multiple_of(index * rows + part * step, step), step)]
        return out.at[pl.ds(part * step, step), cols_at(index, cols)]

    def move(self, p, kind, index, own, target):
        block = self.place(p, index)
        return remote(
            self.source(p) if own else block, block,
            self.sends.at[kind, index, p], self.recvs.at[index, p], "fs", target,
        )

    def arrived(self, p, index):
        self.move(p, 0, index, False, self.f).wait_recv()

    def along_z(self, p, step, index, own, act):
        inside = (self.z < self.nz - 1) if step > 0 else (self.z > 0)

        @pl.when(inside)
        def _():
            act(self.move(p, 0 if step > 0 else 1, index, own, self.f + step * self.ny))

    def along_y(self, p, index, own, act):
        for offset in range(1, self.ny):
            target = self.z * self.ny + lax.rem(self.y + offset, self.ny)
            act(self.move(p, 1 + offset, index, own, target))

    def others(self, zs):
        return [zs * self.ny + lax.rem(self.y + offset, self.ny) for offset in range(1, self.ny)]

    def own(self, act, wait):
        order = range(len(self.pieces))
        for p in order:
            self.along_y(p, self.f, True, act)
            for step in (1, -1):
                self.along_z(p, step, self.f, True, act)
        for p in order:
            if self.pieces[p][5]:
                for index in self.others(self.z):
                    if wait:
                        self.arrived(p, index)
                    for step in (1, -1):
                        self.along_z(p, step, index, False, act)

    def relay(self, distance, act, wait):
        for p in range(len(self.pieces)):
            for step in (1, -1):
                zs = self.z - step * distance

                @pl.when(jnp.logical_and(zs >= 0, zs < self.nz))
                def _():
                    index = zs * self.ny + self.y
                    if wait:
                        self.arrived(p, index)
                    self.along_z(p, step, index, False, act)
                    if not self.pieces[p][5]:
                        self.along_y(p, index, False, act)

        for p in range(len(self.pieces)):
            if self.pieces[p][5]:
                for step in (1, -1):
                    zs = self.z - step * distance

                    @pl.when(jnp.logical_and(zs >= 0, zs < self.nz))
                    def _():
                        for index in self.others(zs):
                            if wait:
                                self.arrived(p, index)
                            self.along_z(p, step, index, False, act)

    def start_own(self):
        self.own(lambda copy: copy.start(), True)

    def start_relay(self, distance):
        self.relay(distance, lambda copy: copy.start(), True)

    def finish(self):
        for p in range(len(self.pieces)):
            if not self.pieces[p][5]:
                for zs in range(self.nz):
                    for index in self.others(zs):
                        self.arrived(p, index)
        self.own(lambda copy: copy.wait_send(), False)
        for distance in range(1, self.nz):
            self.relay(distance, lambda copy: copy.wait_send(), False)

    def greet(self, barrier):
        ny, z, f = self.ny, self.z, self.f
        for index in self.others(z):
            pl.semaphore_signal(barrier, inc=1, device_id={"fs": index}, device_id_type=MESH)

        @pl.when(z > 0)
        def _():
            pl.semaphore_signal(barrier, inc=1, device_id={"fs": f - ny}, device_id_type=MESH)

        @pl.when(z < self.nz - 1)
        def _():
            pl.semaphore_signal(barrier, inc=1, device_id={"fs": f + ny}, device_id_type=MESH)

        ends = (z > 0).astype(jnp.int32) + (z < self.nz - 1).astype(jnp.int32)
        return ends + (ny - 1)

    def own_copies(self, sems):
        return [
            pltpu.make_async_copy(self.source(p), self.place(p, self.f), sems.at[p])
            for p in range(len(self.pieces))
        ]


def greet_tp(ntp, barrier):
    t = lax.axis_index("tp")
    for offset in range(1, ntp):
        pl.semaphore_signal(
            barrier, inc=1, device_id={"tp": lax.rem(t + offset, ntp)}, device_id_type=MESH
        )


def entry_kernel(
    nfs, ntp, ny, pieces,
    gate, up, down, tok, gains,
    gate_out, up_out, down_out, tok_out, gains_out,
    own_sem, send_sem, recv_sem, tok_own, tok_send, tok_fwd, tok_recv,
    gain_own, gain_send, gain_fwd, gain_recv,
):
    shards = ((gate, gate_out, 0), (up, up_out, 0), (down, down_out, 1))
    parts = [(*shard, half, 2, i == 0 and half == 0) for i, shard in enumerate(shards) for half in range(2)]
    weights = FsGather(nfs, ny, parts, send_sem, recv_sem)
    barrier = pltpu.get_barrier_semaphore()
    greet_tp(ntp, barrier)
    pl.semaphore_wait(barrier, weights.greet(barrier) + (ntp - 1))
    toks = TpGather(ntp, tok, tok_out, tok_send, tok_fwd, tok_recv, pieces)
    gain = TpGather(ntp, gains, gains_out, gain_send, gain_fwd, gain_recv, 1)
    copies = weights.own_copies(own_sem)
    copies.append(pltpu.make_async_copy(tok, tok_out.at[:, cols_at(toks.t, toks.width)], tok_own))
    copies.append(
        pltpu.make_async_copy(gains, gains_out.at[:, cols_at(gain.t, gain.width)], gain_own)
    )
    gain.start(0)
    for piece in range(pieces):
        toks.start(piece)
    weights.start_own()
    for copy in copies:
        copy.start()
    for distance in range(1, weights.nz):
        weights.start_relay(distance)
        if distance == 1:
            gain.relay()
            toks.relay()
    for copy in copies:
        copy.wait()
    gain.finish()
    toks.finish()
    weights.finish()


def reduce_kernel(
    nfs, ntp, ny, pieces, factor, gather, dims,
    part, res, scale, *refs,
):
    count = len(dims)
    shards, refs = refs[:count], refs[count:]
    if count:
        wholes = refs[2 : 2 + count]
        refs, (w_own, w_send, w_recv) = refs[:2] + refs[2 + count : -3], refs[-3:]
    if gather:
        (out, full, one, pair, two, s1, v1, s2, v2, own_sem, g_send, g_fwd, g_recv) = refs
    else:
        (out, one, pair, two, s1, v1, s2, v2) = refs
    t = lax.axis_index("tp")
    nx = ntp // 2
    core, chip = lax.rem(t, 2), lax.div(t, 2)
    partner = chip * 2 + (1 - core)
    width = res.shape[1]
    rows = res.shape[0] // pieces

    def at(piece):
        return pl.ds(piece * rows, rows)

    def along_x(offset, which):
        return lax.rem(chip + offset, nx) * 2 + which

    def to_partner(offset, piece):
        return remote(
            part.at[at(piece), cols_at(along_x(offset, 1 - core), width)],
            one.at[offset, at(piece)],
            s1.at[offset, piece], v1.at[offset, piece], "tp", partner,
        )

    def across(offset, piece):
        return remote(
            pair.at[offset - 1, at(piece)],
            two.at[offset - 1, at(piece)],
            s2.at[offset - 1, piece], v2.at[offset - 1, piece], "tp", along_x(offset, core),
        )

    barrier = pltpu.get_barrier_semaphore()
    greet_tp(ntp, barrier)
    if count:
        parts = [(shards[i], wholes[i], dims[i], 0, 1, i == 0) for i in range(count)]
        weights = FsGather(nfs, ny, parts, w_send, w_recv)
        pl.semaphore_wait(barrier, weights.greet(barrier) + (ntp - 1))
    else:
        pl.semaphore_wait(barrier, ntp - 1)
    for piece in range(pieces):
        for offset in range(1, nx):
            to_partner(offset, piece).start()
    for piece in range(pieces):
        to_partner(0, piece).start()
    if count:
        weights.start_own()
        copies = weights.own_copies(w_own)
        for copy in copies:
            copy.start()
    for piece in range(pieces):
        for offset in range(1, nx):
            to_partner(offset, piece).wait_recv()
            mine = part[at(piece), cols_at(along_x(offset, core), width)].astype(F32)
            total = mine + one[offset, at(piece)].astype(F32)
            pair[offset - 1, at(piece)] = total.astype(BF16)
            across(offset, piece).start()
    if gather:
        spread = TpGather(ntp, out, full, g_send, g_fwd, g_recv, pieces)
    for piece in range(pieces):
        to_partner(0, piece).wait_recv()
        total = part[at(piece), cols_at(t, width)].astype(F32) + one[0, at(piece)].astype(F32)
        for offset in range(1, nx):
            across(offset, piece).wait_recv()
            total = total + two[offset - 1, at(piece)].astype(F32)
        value = res[at(piece)].astype(F32) + factor * total * scale[...]
        out[at(piece)] = value.astype(BF16)
        if gather:
            spread.start(piece)
    if gather:
        own = pltpu.make_async_copy(out, full.at[:, cols_at(t, width)], own_sem)
        own.start()
        if count:
            weights.start_relay(1)
        spread.relay()
        if count:
            for distance in range(2, weights.nz):
                weights.start_relay(distance)
        spread.finish()
        own.wait()
    if count:
        for copy in copies:
            copy.wait()
        weights.finish()
    for piece in range(pieces):
        for offset in range(nx):
            to_partner(offset, piece).wait_send()
        for offset in range(1, nx):
            across(offset, piece).wait_send()


def retain_kernel(rate, query, key, value, outgate, cosines, sines, gain, out):
    length, width = query.shape
    even = lax.rem(lax.broadcasted_iota(jnp.int32, (length, width), 1), 2) == 0

    def turned(ref):
        v = ref[...].astype(F32)
        swapped = jnp.where(even, -pltpu.roll(v, width - 1, 1), pltpu.roll(v, 1, 1))
        return v * cosines[...] + swapped * sines[...]

    q = turned(query).astype(BF16)
    k = (turned(key) * width ** -0.5).astype(BF16)
    scores = lax.dot_general(q, k, (((1,), (1,)), ((), ())), preferred_element_type=F32)
    distance = lax.broadcasted_iota(jnp.int32, (length, length), 0) - lax.broadcasted_iota(
        jnp.int32, (length, length), 1
    )
    decay = jnp.exp(-rate[pl.program_id(0), 0] * jnp.maximum(distance, 0).astype(F32))
    scores = jnp.where(distance >= 0, scores * decay, 0.0).astype(BF16)
    kept = jnp.dot(scores, value[...], preferred_element_type=F32)
    kept = kept * lax.rsqrt(jnp.mean(kept * kept, axis=1, keepdims=True) + HEAD_EPS)
    g = outgate[...].astype(F32)
    out[...] = (kept * gain[...] * (g / (1.0 + jnp.exp(-g)))).astype(BF16)


def vmem():
    return pl.BlockSpec(memory_space=pltpu.VMEM)


def anywhere():
    return pl.BlockSpec(memory_space=pl.ANY)


def dma(*shape):
    return pltpu.SemaphoreType.DMA(shape)


def cost(flops):
    return pl.CostEstimate(flops=flops, bytes_accessed=2**20, transcendentals=0)


def along_y_of(nfs, ntp):
    return ntp // 2 if nfs % (ntp // 2) == 0 else 1


def enter(nfs, ntp, gate, up, down, tok, gains):
    ny, nx = along_y_of(nfs, ntp), ntp // 2
    pieces = tok.shape[0] // LEN
    shape = jax.ShapeDtypeStruct
    return pl.pallas_call(
        functools.partial(entry_kernel, nfs, ntp, ny, pieces),
        out_shape=(
            shape((gate.shape[0] * nfs, gate.shape[1]), BF16),
            shape((up.shape[0] * nfs, up.shape[1]), BF16),
            shape((down.shape[0], down.shape[1] * nfs), BF16),
            shape((tok.shape[0], tok.shape[1] * ntp), BF16),
            shape((gains.shape[0], gains.shape[1] * ntp), F32),
        ),
        in_specs=[vmem()] * 5,
        out_specs=(anywhere(),) * 5,
        scratch_shapes=[
            dma(6), dma(ny + 1, nfs, 6), dma(nfs, 6),
            dma(), dma(nx, pieces), dma(nx, pieces), dma(ntp, pieces),
            dma(), dma(nx, 1), dma(nx, 1), dma(ntp, 1),
        ],
        compiler_params=pltpu.CompilerParams(collective_id=0, has_side_effects=True),
        cost_estimate=cost(10**11),
        name="enter",
    )(gate, up, down, tok, gains)


def combine(nfs, ntp, identity, factor, gather, part, res, scale, shards=(), dims=()):
    ny, count = along_y_of(nfs, ntp), len(dims)
    pieces = res.shape[0] // LEN
    nx = ntp // 2
    rows, width = res.shape
    shape = jax.ShapeDtypeStruct
    out_shape = [shape((rows, width), BF16)]
    out_specs = [vmem()]
    scratch = [
        pltpu.VMEM((nx, rows, width), BF16),
        pltpu.VMEM((max(nx - 1, 1), rows, width), BF16),
        pltpu.VMEM((max(nx - 1, 1), rows, width), BF16),
        dma(nx, pieces), dma(nx, pieces),
        dma(max(nx - 1, 1), pieces), dma(max(nx - 1, 1), pieces),
    ]
    if gather:
        out_shape.append(shape((rows, width * ntp), BF16))
        out_specs.append(anywhere())
        scratch += [dma(), dma(nx, pieces), dma(nx, pieces), dma(ntp, pieces)]
    if count:
        for shard, dim in zip(shards, dims):
            grown = [size * (nfs if axis == dim else 1) for axis, size in enumerate(shard.shape)]
            out_shape.append(shape(tuple(grown), BF16))
            out_specs.append(anywhere())
        scratch += [dma(count), dma(ny + 1, nfs, count), dma(nfs, count)]
    return pl.pallas_call(
        functools.partial(reduce_kernel, nfs, ntp, ny, pieces, factor, gather, dims),
        out_shape=tuple(out_shape),
        in_specs=[vmem()] * (3 + count),
        out_specs=tuple(out_specs),
        scratch_shapes=scratch,
        compiler_params=pltpu.CompilerParams(collective_id=identity, has_side_effects=True),
        cost_estimate=cost(4 * 10**10),
        name="combine",
    )(part, res, scale, *shards)


def tables(length, width):
    freq = np.float32(1.0) / np.float32(10000.0) ** np.linspace(0.0, 1.0, width // 2, dtype=np.float32)
    angles = np.arange(length, dtype=np.float32)[:, None] * np.repeat(freq, 2)[None, :]
    return jnp.asarray(np.cos(angles)), jnp.asarray(np.sin(angles))


def retain(query, key, value, outgate, decay_rate, ret_gain):
    heads = decay_rate.shape[0]
    width = query.shape[1] // heads
    cosines, sines = tables(LEN, width)
    block = pl.BlockSpec((LEN, width), lambda h, s: (s, h))
    whole = pl.BlockSpec((LEN, width), lambda h, s: (0, 0))
    return pl.pallas_call(
        retain_kernel,
        grid=(heads, query.shape[0] // LEN),
        out_shape=jax.ShapeDtypeStruct(query.shape, BF16),
        in_specs=[
            pl.BlockSpec(memory_space=pltpu.SMEM), block, block, block, block, whole, whole,
            pl.BlockSpec((1, width), lambda h, s: (0, h)),
        ],
        out_specs=block,
        cost_estimate=cost(10**10),
        name="retain",
    )(decay_rate[:, None], query, key, value, outgate, cosines, sines, ret_gain[None])


def normed(full, gain):
    widened = full.astype(F32)
    mean = jnp.mean(widened * widened, axis=1, keepdims=True)
    return (widened * lax.rsqrt(mean + EPS) * gain).astype(BF16)


def dot(left, right):
    return jnp.dot(left, right, preferred_element_type=F32)


def ffn_part(features, gate, up, down, scale_gate, scale_up):
    hidden = jax.nn.silu(dot(features, gate) * scale_gate) * (dot(features, up) * scale_up)
    return dot(hidden.astype(BF16), down).astype(BF16)


def per_device(
    nfs, ntp,
    tokens, gain_one, w_gate, w_up, w_down, scale_gate, scale_up, scale_down,
    gain_mix, w_query, w_key, w_value, w_outgate,
    scale_query, scale_key, scale_value, scale_outgate,
    ret_gain, decay_rate, w_mix, scale_mix, gain_two,
):
    shards = [w.astype(BF16) for w in (w_query, w_key, w_value, w_outgate, w_mix)]
    gains = jnp.pad(jnp.stack((gain_one, gain_mix, gain_two)), ((0, 5), (0, 0)))
    gate, up, down, full, gains = enter(
        nfs, ntp, w_gate.astype(BF16), w_up.astype(BF16), w_down.astype(BF16), tokens, gains
    )
    part = ffn_part(normed(full, gains[0]), gate, up, down, scale_gate, scale_up)
    first, full, *weights, mix = combine(
        nfs, ntp, 1, 0.5, True, part, tokens, scale_down[None], shards, (0, 0, 0, 0, 1)
    )
    features = normed(full, gains[1])
    scales = (scale_query, scale_key, scale_value, scale_outgate)
    rows = [(dot(features, w) * s).astype(BF16) for w, s in zip(weights, scales)]
    mixed = retain(*rows, decay_rate, ret_gain)
    part = dot(mixed, mix).astype(BF16)
    second, full = combine(nfs, ntp, 2, 1.0, True, part, first, scale_mix[None])
    part = ffn_part(normed(full, gains[2]), gate, up, down, scale_gate, scale_up)
    return combine(nfs, ntp, 3, 0.5, False, part, second, scale_down[None])[0]


def solution(mesh):
    return jax.shard_map(
        functools.partial(per_device, mesh.shape["fs"], mesh.shape["tp"]),
        mesh=mesh,
        in_specs=(
            P("fs", "tp"),
            P("tp"),
            P("fs", "tp"),
            P("fs", "tp"),
            P("tp", "fs"),
            P("tp"),
            P("tp"),
            P("tp"),
            P("tp"),
            P("fs", "tp"),
            P("fs", "tp"),
            P("fs", "tp"),
            P("fs", "tp"),
            P("tp"),
            P("tp"),
            P("tp"),
            P("tp"),
            P("tp"),
            P("tp"),
            P("tp", "fs"),
            P("tp"),
            P("tp"),
        ),
        out_specs=P("fs", "tp"),
        check_vma=False,
    )
```

profile of v0, /device:TPU:0, one launch (start us, length us, event | category | flops | bytes accessed | tf_op | source)
XLA Modules:
  0.0 362.5 jit_solution(18290848518335013200)
XLA Ops:
  0.0 2.0 convert_element_type.71.gate
  2.0 2.0 convert_element_type.72.up
  3.9 1.9 convert_element_type.73.down
  6.5 99.9 %enter.1 = (bf16[2048,768]{1,0:T(8,128)(2,1)}, bf16[2048,768]{1,0:T(8,128)(2,1)}, bf16[768,2048]{1,0:T(8,128)(2,1)}, bf16[768,2048]{1,0:T(8,128)(2,1)}, f32[8,2048]{1,0:T(8,128)}) custom-call(bf16[256,768]{1,0:T(8,128)(2,1)} %convert_element_type.71.gate, bf16[256,768]{1,0:T(8,128)(2,1)} %convert_element_type.72.up, ...), custom_call_target="tpu_custom_call" | custom-call | flops 99999997952 | bytes 1048576 | tf_op jit(solution)/shard_map/enter/pallas_call | solution.py:435
  107.5 2.6 fusion
  110.1 5.9 %fusion.15 = f32[768,768]{1,0:T(8,128)} fusion(bf16[2048,768]{1,0:T(8,128)(2,1)} %get-tuple-element.21, bf16[768,2048]{1,0:T(8,128)(2,1)S(1)} %copy-done.1, f32[2048]{0:T(1024)S(1)} %bitcast.28, f32[768]{0:T(1024)S(1)} %add_rsqrt_fusion.2), kind=kOutput, calls=%fused_computation.25 | convolution fusion | flops 2422210560 | bytes 8662016 | tf_op jit(solution)/shard_map/dot_general | solution.py:527
  116.0 11.1 %convolution_convert_fusion.2.part = bf16[768,2048]{1,0:T(8,128)(2,1)} fusion(bf16[768,2048]{1,0:T(8,128)(2,1)} %get-tuple-element.23, f32[768,768]{1,0:T(8,128)} %fusion.15, bf16[2048,768]{1,0:T(8,128)(2,1)} %get-tuple-element.22, f32[768]{0:T(1024)S(1)} %copy-done.7, f32[768]{0:T(1024)S(1)} %copy-done.8, bf16[768,2048]{1,0:T(8,128)(2,1)S(1)} %copy-done.1, ...), kind=kOutput, calls=%fused_computation.17 | convolution fusion | flops 4844421120 | bytes 14959616 | tf_op jit(solution)/shard_map/dot_general | solution.py:527
  127.1 1.8 convert_element_type.78.refs_0_
  128.9 1.8 convert_element_type.79.refs_1_
  130.7 1.8 convert_element_type.80.refs_2_
  135.0 109.6 %combine.3 = (bf16[768,512]{1,0:T(8,128)(2,1)}, bf16[768,2048]{1,0:T(8,128)(2,1)}, bf16[2048,512]{1,0:T(8,128)(2,1)}, bf16[2048,512]{1,0:T(8,128)(2,1)}, bf16[20...) custom-call(bf16[768,2048]{1,0:T(8,128)(2,1)} %convolution_convert_fusion.2.part, ...), custom_call_target="tpu_custom_call" | custom-call | flops 40000000000 | bytes 1048576 | tf_op jit(solution)/shard_map/combine/pallas_call | solution.py:482
  244.7 2.7 fusion.3
  247.5 4.5 %multiply_convert_fusion.2.outgate = bf16[768,512]{1,0:T(8,128)(2,1)} fusion(bf16[2048,512]{1,0:T(8,128)(2,1)} %get-tuple-element.28, f32[512]{0:T(512)S(1)} %copy-done.9, bf16[768,2048]{1,0:T(8,128)(2,1)S(1)} %copy-done, f32[2048]{0:T(1024)S(1)} %bitcast.24, f32[768]{0:T(1024)S(1)} %add_rsqrt_fusion.1), kind=kOutput, calls=%fused_computation.20 | convolution fusion | flops 1617690624 | bytes 6042624 | tf_op jit(solution)/shard_map/dot_general | solution.py:527
  252.0 2.8 multiply_convert_fusion.3.value
  254.8 2.7 multiply_convert_fusion.4.key
  257.5 2.7 multiply_convert_fusion.5.query
  260.9 7.1 %retain.1 = bf16[768,512]{1,0:T(8,128)(2,1)} custom-call(f32[2,1]{1,0:T(2,128)} %copy.25.rate, bf16[768,512]{1,0:T(8,128)(2,1)} %multiply_convert_fusion.5.query, bf16[768,512]{1,0:T(8,128)(2,1)} %multiply_convert_fusion.4.key, bf16[768,512]{1,0:T(8,128)(2,1)} %multiply_convert_fusion.3.value, bf16[768,512]{1,0:T(8,128)(2,1)} %multiply_convert_fusion.2.outgate, ...), custom_call_target="tpu_custom_call" | custom-call | flops 10000000000 | bytes 1048576 | tf_op jit(solution)/shard_map/retain/pallas_call | solution.py:506
  268.0 4.6 %convolution_convert_fusion.part = bf16[768,2048]{1,0:T(8,128)(2,1)} fusion(bf16[768,512]{1,0:T(8,128)(2,1)} %retain.1, bf16[512,2048]{1,0:T(8,128)(2,1)S(1)} %copy-done.14), kind=kOutput, calls=%fused_computation.15 | convolution fusion | flops 1612185600 | bytes 6029312 | tf_op jit(solution)/shard_map/dot_general | solution.py:527
  272.6 43.3 %combine.4 = (bf16[768,512]{1,0:T(8,128)(2,1)}, bf16[768,2048]{1,0:T(8,128)(2,1)}) custom-call(bf16[768,2048]{1,0:T(8,128)(2,1)} %convolution_convert_fusion.part, bf16[768,512]{1,0:T(8,128)(2,1)} %get-tuple-element.30.res, f32[1,512]{1,0:T(1,128)} %bitcast.34), custom_call_target="tpu_custom_call" | custom-call | flops 40000000000 | bytes 1048576 | tf_op jit(solution)/shard_map/combine/pallas_call | solution.py:482
  315.9 2.7 fusion.6
  318.7 5.9 %fusion.10 = f32[768,768]{1,0:T(8,128)} fusion(bf16[2048,768]{1,0:T(8,128)(2,1)} %get-tuple-element.21, bf16[768,2048]{1,0:T(8,128)(2,1)S(1)} %copy-done.2, f32[2048]{0:T(1024)S(1)} %bitcast.22, f32[768]{0:T(1024)S(1)} %add_rsqrt_fusion), kind=kOutput, calls=%fused_computation.24 | convolution fusion | flops 2422210560 | bytes 8662016 | tf_op jit(solution)/shard_map/dot_general | solution.py:527
  324.6 11.1 %convolution_convert_fusion.1.part = bf16[768,2048]{1,0:T(8,128)(2,1)} fusion(bf16[768,2048]{1,0:T(8,128)(2,1)} %get-tuple-element.23, f32[768,768]{1,0:T(8,128)} %fusion.10, bf16[2048,768]{1,0:T(8,128)(2,1)} %get-tuple-element.22, f32[768]{0:T(1024)S(1)} %copy-done.7, f32[768]{0:T(1024)S(1)} %copy-done.8, bf16[768,2048]{1,0:T(8,128)(2,1)S(1)} %copy-done.2, ...), kind=kOutput, calls=%fused_computation.16 | convolution fusion | flops 4844421120 | bytes 14959616 | tf_op jit(solution)/shard_map/dot_general | solution.py:527
  335.8 24.7 %combine.5 = bf16[768,512]{1,0:T(8,128)(2,1)} custom-call(bf16[768,2048]{1,0:T(8,128)(2,1)} %convolution_convert_fusion.1.part, bf16[768,512]{1,0:T(8,128)(2,1)} %get-tuple-element.32.res, f32[1,512]{1,0:T(1,128)} %bitcast.36), custom_call_target="tpu_custom_call" | custom-call | flops 40000000000 | bytes 1048576 | tf_op jit(solution)/shard_map/combine/pallas_call | solution.py:482
  360.4 2.1 copy.27
  (44 shorter events, 5.1 us)
Async XLA Ops:
  0.0 5.9 %copy-start.6 = (f32[512]{0:T(512)S(1)}, f32[512]{0:T(512)}, u32[]{:S(2)}) copy-start(f32[512]{0:T(512)} %param.25) | copy-start | bytes 6148
  0.0 5.9 %copy-start.5 = (f32[512]{0:T(512)S(1)}, f32[512]{0:T(512)}, u32[]{:S(2)}) copy-start(f32[512]{0:T(512)} %param.32) | copy-start | bytes 6148
  0.0 5.9 %copy-start.4 = (f32[512]{0:T(512)S(1)}, f32[512]{0:T(512)}, u32[]{:S(2)}) copy-start(f32[512]{0:T(512)} %param.45) | copy-start | bytes 6148
  106.4 3.7 %copy-start.1 = (bf16[768,2048]{1,0:T(8,128)(2,1)S(1)}, bf16[768,2048]{1,0:T(8,128)(2,1)}, u32[]{:S(2)}) copy-start(bf16[768,2048]{1,0:T(8,128)(2,1)} %get-tuple-element.19) | copy-start | bytes 9437188
  110.1 6.0 %copy-start.7 = (f32[768]{0:T(1024)S(1)}, f32[768]{0:T(1024)}, u32[]{:S(2)}) copy-start(f32[768]{0:T(1024)} %param.30) | copy-start | bytes 9220
  110.1 6.0 %copy-start.8 = (f32[768]{0:T(1024)S(1)}, f32[768]{0:T(1024)}, u32[]{:S(2)}) copy-start(f32[768]{0:T(1024)} %param.29) | copy-start | bytes 9220
  127.1 7.2 %copy-start.3 = (f32[512,256]{1,0:T(8,128)S(1)}, f32[512,256]{1,0:T(8,128)}, u32[]{:S(2)}) copy-start(f32[512,256]{1,0:T(8,128)} %param.43) | copy-start | bytes 1572868
  244.7 2.8 copy-start
  244.7 2.8 copy-start.9
  247.5 4.5 %copy-start.10 = (f32[512]{0:T(512)S(1)}, f32[512]{0:T(512)}, u32[]{:S(2)}) copy-start(f32[512]{0:T(512)} %param.39) | copy-start | bytes 6148
  247.5 4.5 %copy-start.17 = (bf16[2048,512]{1,0:T(8,128)(2,1)S(1)}, bf16[2048,512]{1,0:T(8,128)(2,1)}, u32[]{:S(2)}) copy-start(bf16[2048,512]{1,0:T(8,128)(2,1)} %get-tuple-element.27) | copy-start | bytes 6291460
  252.0 2.8 copy-start.11
  252.0 2.8 copy-start.16
  254.8 2.8 copy-start.12
  254.8 2.8 copy-start.15
  257.5 2.7 copy-start.13
  260.9 7.1 %copy-start.14 = (bf16[512,2048]{1,0:T(8,128)(2,1)S(1)}, bf16[512,2048]{1,0:T(8,128)(2,1)}, u32[]{:S(2)}) copy-start(bf16[512,2048]{1,0:T(8,128)(2,1)} %get-tuple-element.29) | copy-start | bytes 6291460
  315.9 2.8 copy-start.2
where the time goes:
time: 363 us; the launch traced here: 362 us
  Pallas kernels  285 us (79%)
  matrix products  51.3 us (14%)
  other arithmetic  22.4 us (6%)
  local copies, waits for them, and re-layouts  3.99 us (1%)
    pallas_call x3, Pallas kernels, combine(): pl.pallas_call(functools.partial(reduce_kernel, nfs, ntp, ny, pieces, fac...  178 us
    pallas_call x1, Pallas kernels, enter(): pl.pallas_call(functools.partial(entry_kernel, nfs, ntp, ny, pieces), out...  99.9 us
    dot_general x9, matrix products, dot(): return jnp.dot(left, right, preferred_element_type=F32)  51.3 us
    reduce_sum x3, other arithmetic, normed(): mean = jnp.mean(widened * widened, axis=1, keepdims=True)  8.01 us
    convert_element_type x5, other arithmetic, per_device(): w.astype(BF16)  7.93 us

commit v1 on v0

v1 whole, which is shorter than its diff:
```python
import functools
from types import SimpleNamespace

import jax
import jax.numpy as jnp
import numpy as np
from jax import lax
from jax.experimental import pallas as pl
from jax.experimental.pallas import tpu as pltpu
from jax.sharding import PartitionSpec as P

LEN = 256
EPS = 1e-06
HEAD_EPS = 0.1
MESH = pl.DeviceIdType.MESH
BF16 = jnp.bfloat16
F32 = jnp.float32
WEIGHTS = ("gate", "up", "down", "query", "key", "value", "outgate", "mix")
DIMS = (0, 0, 1, 0, 0, 0, 0, 1)
PARTS = (2, 2, 2, 1, 1, 1, 1, 2)
ALONG_Z = ((0, 0), (3, 0))


def cols_at(index, width):
    return pl.ds(pl.multiple_of(index * width, width), width)


def remote(src, dst, send_sem, recv_sem, axis, target):
    return pltpu.make_async_remote_copy(
        src_ref=src,
        dst_ref=dst,
        send_sem=send_sem,
        recv_sem=recv_sem,
        device_id={axis: target},
        device_id_type=MESH,
    )


def dot(left, right):
    return jnp.dot(left, right, preferred_element_type=F32)


class TpGroup:
    def __init__(self, ntp):
        self.ntp, self.nx = ntp, ntp // 2
        self.t = lax.axis_index("tp")
        self.core, self.chip = lax.rem(self.t, 2), lax.div(self.t, 2)
        self.partner = self.chip * 2 + (1 - self.core)

    def along_x(self, offset, core):
        return lax.rem(self.chip + offset, self.nx) * 2 + core

    def greet(self, barrier):
        for offset in range(1, self.ntp):
            target = lax.rem(self.t + offset, self.ntp)
            pl.semaphore_signal(barrier, inc=1, device_id={"tp": target}, device_id_type=MESH)
        return self.ntp - 1


class TpGather:
    def __init__(self, group, src, out, sems, rows):
        self.group = group
        self.src, self.out, self.rows = src, out, rows
        self.sends, self.forwards, self.recvs = sems
        self.width = src.shape[1]

    def at(self, piece):
        return pl.ds(piece * self.rows, self.rows)

    def place(self, index, piece):
        return self.out.at[self.at(piece), cols_at(index, self.width)]

    def own_sends(self, piece):
        group = self.group
        copies = []
        for offset in range(group.nx - 1, -1, -1):
            target = group.along_x(offset, group.core) if offset else group.partner
            copies.append(
                remote(
                    self.src.at[self.at(piece)], self.place(group.t, piece),
                    self.sends.at[offset, piece], self.recvs.at[group.t, piece], "tp", target,
                )
            )
        return copies

    def forward(self, offset, piece):
        group = self.group
        index = group.along_x(group.nx - offset, group.core)
        block = self.place(index, piece)
        return remote(
            block, block, self.forwards.at[offset, piece], self.recvs.at[index, piece],
            "tp", group.partner,
        )

    def arrived(self, index, piece):
        block = self.place(index, piece)
        remote(
            block, block, self.sends.at[0, piece], self.recvs.at[index, piece],
            "tp", self.group.partner,
        ).wait_recv()

    def start(self, piece):
        for copy in self.own_sends(piece):
            copy.start()

    def relay(self, piece):
        group = self.group
        for offset in range(1, group.nx):
            self.arrived(group.along_x(group.nx - offset, group.core), piece)
            self.forward(offset, piece).start()

    def complete(self, piece):
        group = self.group
        for offset in range(group.nx):
            self.arrived(group.along_x(offset, 1 - group.core), piece)
        for offset in range(1, group.nx):
            self.forward(offset, piece).wait_send()

    def finish(self, piece):
        for copy in self.own_sends(piece):
            copy.wait_send()


class TpReduce:
    def __init__(self, group, part, pair, one, two, sems, rows, width):
        self.group, self.part, self.pair, self.one, self.two = group, part, pair, one, two
        self.s1, self.v1, self.s2, self.v2 = sems
        self.rows, self.width = rows, width

    def at(self, piece):
        return pl.ds(piece * self.rows, self.rows)

    def block(self, offset, core):
        return cols_at(self.group.along_x(offset, core), self.width)

    def to_partner(self, offset, piece):
        return remote(
            self.part.at[self.at(piece), self.block(offset, 1 - self.group.core)],
            self.one.at[offset, self.at(piece)],
            self.s1.at[offset, piece], self.v1.at[offset, piece], "tp", self.group.partner,
        )

    def across(self, offset, piece):
        return remote(
            self.pair.at[offset - 1, self.at(piece)],
            self.two.at[offset - 1, self.at(piece)],
            self.s2.at[offset - 1, piece], self.v2.at[offset - 1, piece],
            "tp", self.group.along_x(offset, self.group.core),
        )

    def start(self, piece):
        for offset in range(self.group.nx - 1, -1, -1):
            self.to_partner(offset, piece).start()

    def cross(self, piece):
        at = self.at(piece)
        for offset in range(self.group.nx - 1, 0, -1):
            self.to_partner(offset, piece).wait_recv()
            mine = self.part[at, self.block(offset, self.group.core)].astype(F32)
            self.pair[offset - 1, at] = (mine + self.one[offset, at].astype(F32)).astype(BF16)
            self.across(offset, piece).start()

    def total(self, piece):
        at = self.at(piece)
        self.to_partner(0, piece).wait_recv()
        value = self.part[at, self.block(0, self.group.core)].astype(F32)
        value = value + self.one[0, at].astype(F32)
        for offset in range(1, self.group.nx):
            self.across(offset, piece).wait_recv()
            value = value + self.two[offset - 1, at].astype(F32)
        return value

    def finish(self, piece):
        for offset in range(self.group.nx):
            self.to_partner(offset, piece).wait_send()
        for offset in range(1, self.group.nx):
            self.across(offset, piece).wait_send()


class FsStream:
    def __init__(self, nfs, ny, pieces, sends, recvs):
        self.ny, self.nz = ny, nfs // ny
        self.f = lax.axis_index("fs")
        self.z, self.y = lax.div(self.f, ny), lax.rem(self.f, ny)
        self.pieces = pieces
        self.sends, self.recvs = sends, recvs
        self.events, self.done = self.schedule(), 0

    def whole_z(self, p):
        return self.pieces[p].along_z

    def place(self, p, index):
        piece = self.pieces[p]
        if piece.dim == 0:
            start = pl.multiple_of(index * piece.rows + piece.start, 16)
            return piece.buf.at[pl.ds(start, piece.size)]
        return piece.buf.at[pl.ds(piece.start, piece.size), cols_at(index, piece.cols)]

    def move(self, p, kind, index, target):
        block = self.place(p, index)
        return remote(
            block, block, self.sends.at[kind, index, p], self.recvs.at[index, p], "fs", target
        )

    def arrived(self, p, index):
        self.move(p, 0, index, self.f).wait_recv()

    def move_z(self, p, step, index, act):
        inside = (self.z < self.nz - 1) if step > 0 else (self.z > 0)

        @pl.when(inside)
        def _():
            act(self.move(p, 0 if step > 0 else 1, index, self.f + step * self.ny))

    def move_y(self, p, index, act):
        for offset in range(1, self.ny):
            target = self.z * self.ny + lax.rem(self.y + offset, self.ny)
            act(self.move(p, 1 + offset, index, target))

    def others(self, zs):
        return [zs * self.ny + lax.rem(self.y + offset, self.ny) for offset in range(1, self.ny)]

    def own(self, p, act, wait):
        self.move_y(p, self.f, act)
        for step in (1, -1):
            self.move_z(p, step, self.f, act)

    def side(self, p, act, wait):
        for index in self.others(self.z):
            if wait:
                self.arrived(p, index)
            for step in (1, -1):
                self.move_z(p, step, index, act)

    def relay(self, distance, p, act, wait):
        for step in (1, -1):
            zs = self.z - step * distance

            @pl.when(jnp.logical_and(zs >= 0, zs < self.nz))
            def _():
                same = zs * self.ny + self.y
                for index in [same] + (self.others(zs) if self.whole_z(p) else []):
                    if wait:
                        self.arrived(p, index)
                    self.move_z(p, step, index, act)
                    if not self.whole_z(p):
                        self.move_y(p, index, act)

    def schedule(self):
        count = len(self.pieces)
        events = [(-1, functools.partial(self.own, 0))]
        for tick in range(count + self.nz - 2):
            if tick + 1 < count:
                events.append((tick, functools.partial(self.own, tick + 1)))
            if tick < count and self.whole_z(tick):
                events.append((tick, functools.partial(self.side, tick)))
            for distance in range(1, self.nz):
                if 0 <= tick + 1 - distance < count:
                    events.append((tick, functools.partial(self.relay, distance, tick + 1 - distance)))
        return events

    def some(self, count):
        for _, event in self.events[self.done : self.done + count]:
            event(lambda copy: copy.start(), True)
        self.done = min(self.done + count, len(self.events))

    def upto(self, tick):
        ahead = sum(1 for at, _ in self.events[self.done :] if at <= tick)
        self.some(ahead)

    def need(self, p):
        self.upto(p + self.nz - 2)
        if not self.whole_z(p):
            for zs in range(self.nz):
                for index in self.others(zs):
                    self.arrived(p, index)

    def finish(self):
        for _, event in self.events:
            event(lambda copy: copy.wait_send(), False)

    def greet(self, barrier):
        ny, z, f = self.ny, self.z, self.f
        for index in self.others(z):
            pl.semaphore_signal(barrier, inc=1, device_id={"fs": index}, device_id_type=MESH)

        @pl.when(z > 0)
        def _():
            pl.semaphore_signal(barrier, inc=1, device_id={"fs": f - ny}, device_id_type=MESH)

        @pl.when(z < self.nz - 1)
        def _():
            pl.semaphore_signal(barrier, inc=1, device_id={"fs": f + ny}, device_id_type=MESH)

        ends = (z > 0).astype(jnp.int32) + (z < self.nz - 1).astype(jnp.int32)
        return ends + (ny - 1)


def layer_kernel(nfs, ntp, ny, names, *refs):
    r = SimpleNamespace(**dict(zip(names, refs)))
    rows, width = r.tok.shape
    count = rows // LEN
    chunks = range(count)
    group = TpGroup(ntp)
    shards = [getattr(r, "w_" + name) for name in WEIGHTS]
    wholes = [getattr(r, name) for name in WEIGHTS]
    pieces, first_of = [], {}
    for i, name in enumerate(WEIGHTS):
        first_of[name] = len(pieces)
        size = shards[i].shape[0] // PARTS[i]
        for part in range(PARTS[i]):
            pieces.append(
                SimpleNamespace(
                    buf=wholes[i], dim=DIMS[i], rows=shards[i].shape[0], cols=shards[i].shape[1],
                    start=part * size, size=size, along_z=(i, part) in ALONG_Z,
                )
            )
    stream = FsStream(nfs, ny, pieces, r.w_send, r.w_recv)

    def need(name):
        i = WEIGHTS.index(name)
        for part in range(PARTS[i]):
            stream.need(first_of[name] + part)

    def at(c):
        return pl.ds(c * LEN, LEN)

    barrier = pltpu.get_barrier_semaphore()
    greeted = group.greet(barrier) + stream.greet(barrier)
    loads = [
        pltpu.make_async_copy(shards[i], getattr(r, "stage_" + name), r.load_sem.at[i])
        for i, name in enumerate(WEIGHTS)
    ]
    for load in loads:
        load.start()

    def cast(i):
        loads[i].wait()
        shard = shards[i].shape
        value = getattr(r, "stage_" + WEIGHTS[i])[...].astype(BF16)
        if DIMS[i] == 0:
            wholes[i][pl.ds(pl.multiple_of(stream.f * shard[0], shard[0]), shard[0]), :] = value
        else:
            wholes[i][:, cols_at(stream.f, shard[1])] = value

    r.gain_own[...] = jnp.zeros(r.gain_own.shape, F32)
    for row, ref in enumerate((r.gain_one, r.gain_mix, r.gain_two)):
        r.gain_own[row : row + 1, :] = ref[...]
    cast(0)
    cast(1)
    r.full_0[:, cols_at(group.t, width)] = r.tok[...]
    r.gains[:, cols_at(group.t, width)] = r.gain_own[...]
    pl.semaphore_wait(barrier, greeted)

    gain_gather = TpGather(group, r.gain_own, r.gains, (r.n_send, r.n_fwd, r.n_recv), 8)
    gathers = [
        TpGather(group, src, full, (r.g_send.at[i], r.g_fwd.at[i], r.g_recv.at[i]), LEN)
        for i, (src, full) in enumerate(
            ((r.tok, r.full_0), (r.first, r.full_1), (r.second, r.full_2))
        )
    ]
    reduces = [
        TpReduce(
            group, r.part, r.pair, r.one.at[i], r.two.at[i],
            (r.r_s1.at[i], r.r_v1.at[i], r.r_s2.at[i], r.r_v2.at[i]), LEN, width,
        )
        for i in range(3)
    ]
    gain_gather.start(0)
    for c in chunks:
        gathers[0].start(c)
    stream.some(2)
    for i in range(2, len(WEIGHTS)):
        cast(i)

    def norm(full, row, c):
        gain = r.gains[row : row + 1, :]
        step = 32

        def body(i, carry):
            some = pl.ds(pl.multiple_of(c * LEN + i * step, step), step)
            v = full[some, :].astype(F32)
            mean = jnp.mean(v * v, axis=1, keepdims=True)
            full[some, :] = (v * lax.rsqrt(mean + EPS) * gain).astype(BF16)
            return carry

        lax.fori_loop(0, LEN // step, body, 0)

    def gate_up(full, c):
        units = r.gate.shape[1]
        tile = 256 if units % 256 == 0 else 128

        def body(n, carry):
            cols = cols_at(n, tile)
            x = full[at(c), :]
            g = dot(x, r.gate[:, cols]) * r.scale_gate[:, cols]
            u = dot(x, r.up[:, cols]) * r.scale_up[:, cols]
            r.hidden[at(c), cols] = (g / (1.0 + jnp.exp(-g)) * u).astype(BF16)
            return carry

        lax.fori_loop(0, units // tile, body, 0)

    def partial(left, weight, c):
        def body(n, carry):
            cols = cols_at(n, width)
            r.part[at(c), cols] = dot(left[at(c), :], weight[:, cols]).astype(BF16)
            return carry

        lax.fori_loop(0, ntp, body, 0)

    def project(name, full):
        weight, scale, out = getattr(r, name), getattr(r, "scale_" + name), getattr(r, "a_" + name)

        def body(c, carry):
            some = pl.ds(pl.multiple_of(c * LEN, LEN), LEN)
            out[some, :] = (dot(full[some, :], weight[...]) * scale[...]).astype(BF16)
            return carry

        lax.fori_loop(0, count, body, 0)

    def retain():
        heads = r.rate.shape[1]
        size = width // heads
        even = lax.rem(lax.broadcasted_iota(jnp.int32, (LEN, size), 1), 2) == 0
        distance = lax.broadcasted_iota(jnp.int32, (LEN, LEN), 0) - lax.broadcasted_iota(
            jnp.int32, (LEN, LEN), 1
        )

        def body(i, carry):
            c, h = lax.div(i, heads), lax.rem(i, heads)
            some, cols = pl.ds(pl.multiple_of(c * LEN, LEN), LEN), cols_at(h, size)

            def turned(ref):
                v = ref[some, cols].astype(F32)
                swapped = jnp.where(even, -pltpu.roll(v, size - 1, 1), pltpu.roll(v, 1, 1))
                return v * r.cosines[...] + swapped * r.sines[...]

            q = turned(r.a_query).astype(BF16)
            k = (turned(r.a_key) * size ** -0.5).astype(BF16)
            scores = lax.dot_general(q, k, (((1,), (1,)), ((), ())), preferred_element_type=F32)
            decay = jnp.exp(-r.rate[0, h] * jnp.maximum(distance, 0).astype(F32))
            scores = jnp.where(distance >= 0, scores * decay, 0.0).astype(BF16)
            kept = dot(scores, r.a_value[some, cols])
            kept = kept * lax.rsqrt(jnp.mean(kept * kept, axis=1, keepdims=True) + HEAD_EPS)
            g = r.a_outgate[some, cols].astype(F32)
            gated = kept * r.ret_gain[:, cols] * (g / (1.0 + jnp.exp(-g)))
            r.mixed[some, cols] = gated.astype(BF16)
            return carry

        lax.fori_loop(0, count * heads, body, 0)

    def settle(i, c, factor, scale, res, out):
        value = res[at(c), :].astype(F32) + factor * reduces[i].total(c) * scale[...]
        value = value.astype(BF16)
        out[at(c), :] = value
        if i < 2:
            full = (r.full_1, r.full_2)[i]
            full[at(c), cols_at(group.t, width)] = value
            gathers[i + 1].start(c)

    gain_gather.relay(0)
    for c in chunks:
        stream.upto(c)
        gathers[0].relay(c)
    gain_gather.complete(0)
    for c in chunks:
        stream.some(1)
        gathers[0].complete(c)
        norm(r.full_0, 0, c)
    need("gate")
    need("up")
    for c in chunks:
        gate_up(r.full_0, c)
        stream.some(1)
    need("down")
    for c in chunks:
        partial(r.hidden, r.down, c)
        reduces[0].start(c)
        stream.some(1)
    for c in chunks:
        reduces[0].cross(c)
        stream.some(1)
    for c in chunks:
        settle(0, c, 0.5, r.scale_down, r.tok, r.first)
        stream.some(1)
    for c in chunks:
        gathers[1].relay(c)
        stream.some(1)
    for c in chunks:
        gathers[1].complete(c)
        norm(r.full_1, 1, c)
        reduces[0].finish(c)
    for name in ("query", "key", "value", "outgate"):
        need(name)
        project(name, r.full_1)
        stream.some(1)
    retain()
    need("mix")
    for c in chunks:
        partial(r.mixed, r.mix, c)
        reduces[1].start(c)
    for c in chunks:
        reduces[1].cross(c)
    for c in chunks:
        settle(1, c, 1.0, r.scale_mix, r.first, r.second)
    gathers[2].relay(0)
    for c in chunks:
        gathers[2].complete(c)
        norm(r.full_2, 2, c)
        if c > 0:
            reduces[2].cross(c - 1)
        gate_up(r.full_2, c)
        if c + 1 < count:
            gathers[2].relay(c + 1)
        reduces[1].finish(c)
        partial(r.hidden, r.down, c)
        reduces[2].start(c)
    reduces[2].cross(count - 1)
    for c in chunks:
        settle(2, c, 0.5, r.scale_down, r.second, r.out)
    for c in chunks:
        reduces[2].finish(c)
        for gather in gathers:
            gather.finish(c)
    gain_gather.finish(0)
    stream.finish()


def vmem():
    return pl.BlockSpec(memory_space=pltpu.VMEM)


def dma(*shape):
    return pltpu.SemaphoreType.DMA(shape)


def along_y_of(nfs, ntp):
    return ntp // 2 if nfs % (ntp // 2) == 0 else 1


def tables(length, width):
    freq = np.float32(1.0) / np.float32(10000.0) ** np.linspace(0.0, 1.0, width // 2, dtype=np.float32)
    angles = np.arange(length, dtype=np.float32)[:, None] * np.repeat(freq, 2)[None, :]
    return jnp.asarray(np.cos(angles)), jnp.asarray(np.sin(angles))


def per_device(
    nfs, ntp,
    tokens, gain_one, w_gate, w_up, w_down, scale_gate, scale_up, scale_down,
    gain_mix, w_query, w_key, w_value, w_outgate,
    scale_query, scale_key, scale_value, scale_outgate,
    ret_gain, decay_rate, w_mix, scale_mix, gain_two,
):
    ny, nx = along_y_of(nfs, ntp), ntp // 2
    rows, width = tokens.shape
    count = rows // LEN
    model = width * ntp
    weights = (w_gate, w_up, w_down, w_query, w_key, w_value, w_outgate, w_mix)
    cosines, sines = tables(LEN, width // decay_rate.shape[0])
    anywhere = pl.BlockSpec(memory_space=pl.ANY)
    inputs = {"w_" + name: (w, anywhere) for name, w in zip(WEIGHTS, weights)}
    inputs["tok"] = (tokens, vmem())
    inputs["rate"] = (decay_rate[None], pl.BlockSpec(memory_space=pltpu.SMEM))
    inputs["cosines"], inputs["sines"] = (cosines, vmem()), (sines, vmem())
    for name, value in (
        ("gain_one", gain_one), ("gain_mix", gain_mix), ("gain_two", gain_two),
        ("scale_gate", scale_gate), ("scale_up", scale_up), ("scale_down", scale_down),
        ("scale_query", scale_query), ("scale_key", scale_key), ("scale_value", scale_value),
        ("scale_outgate", scale_outgate), ("scale_mix", scale_mix), ("ret_gain", ret_gain),
    ):
        inputs[name] = (value[None], vmem())
    scratch = {}
    for name, w, dim in zip(WEIGHTS, weights, DIMS):
        grown = tuple(size * (nfs if axis == dim else 1) for axis, size in enumerate(w.shape))
        scratch[name] = pltpu.VMEM(grown, BF16)
        scratch["stage_" + name] = pltpu.VMEM(w.shape, F32)
    for i in range(3):
        scratch["full_%d" % i] = pltpu.VMEM((rows, model), BF16)
    scratch["part"] = pltpu.VMEM((rows, model), BF16)
    scratch["hidden"] = pltpu.VMEM((rows, w_gate.shape[1]), BF16)
    far = max(nx - 1, 1)
    scratch["pair"] = pltpu.VMEM((far, rows, width), BF16)
    scratch["one"] = pltpu.VMEM((3, nx, rows, width), BF16)
    scratch["two"] = pltpu.VMEM((3, far, rows, width), BF16)
    for name in ("a_query", "a_key", "a_value", "a_outgate", "mixed", "first", "second"):
        scratch[name] = pltpu.VMEM((rows, width), BF16)
    scratch["gain_own"] = pltpu.VMEM((8, width), F32)
    scratch["gains"] = pltpu.VMEM((8, model), F32)
    total = sum(PARTS)
    scratch["load_sem"] = dma(len(WEIGHTS))
    scratch["w_send"], scratch["w_recv"] = dma(ny + 1, nfs, total), dma(nfs, total)
    scratch["n_send"], scratch["n_fwd"], scratch["n_recv"] = dma(nx, 1), dma(nx, 1), dma(ntp, 1)
    scratch["g_send"], scratch["g_fwd"] = dma(3, nx, count), dma(3, nx, count)
    scratch["g_recv"] = dma(3, ntp, count)
    scratch["r_s1"], scratch["r_v1"] = dma(3, nx, count), dma(3, nx, count)
    scratch["r_s2"], scratch["r_v2"] = dma(3, far, count), dma(3, far, count)
    names = list(inputs) + ["out"] + list(scratch)
    return pl.pallas_call(
        functools.partial(layer_kernel, nfs, ntp, ny, names),
        out_shape=jax.ShapeDtypeStruct((rows, width), BF16),
        in_specs=[spec for _, spec in inputs.values()],
        out_specs=vmem(),
        scratch_shapes=list(scratch.values()),
        compiler_params=pltpu.CompilerParams(
            collective_id=0, has_side_effects=True, vmem_limit_bytes=67043328
        ),
        cost_estimate=pl.CostEstimate(flops=4 * 10**10, bytes_accessed=2**24, transcendentals=0),
        name="layer",
    )(*[value for value, _ in inputs.values()])


def solution(mesh):
    return jax.shard_map(
        functools.partial(per_device, mesh.shape["fs"], mesh.shape["tp"]),
        mesh=mesh,
        in_specs=(
            P("fs", "tp"), P("tp"), P("fs", "tp"), P("fs", "tp"), P("tp", "fs"),
            P("tp"), P("tp"), P("tp"), P("tp"),
            P("fs", "tp"), P("fs", "tp"), P("fs", "tp"), P("fs", "tp"),
            P("tp"), P("tp"), P("tp"), P("tp"), P("tp"), P("tp"),
            P("tp", "fs"), P("tp"), P("tp"),
        ),
        out_specs=P("fs", "tp"),
        check_vma=False,
    )
```

time: 363 us -> 284 us (0.78)
  matrix products: 51.3 us -> 0 us
  other arithmetic: 22.4 us -> 0 us
  Pallas kernels: 285 us -> 280 us
    dot_general x9 -> x0, matrix products: 51.3 us -> none  [dot(): return jnp.dot(left, right, preferred_element_type=F32)]
    convert_element_type x8 -> x0, other arithmetic: 13.8 us -> none  [the longest x5 7.93 us: per_device(): w.astype(BF16)]
    reduce_sum x3 -> x0, other arithmetic: 8.01 us -> none  [normed(): mean = jnp.mean(widened * widened, axis=1, keepdims=True)]
    pallas_call x5 -> x1, Pallas kernels: 285 us -> 280 us  [per_device(): pl.pallas_call(functools.partial(layer_kernel, nfs, ntp, ny, names), out_...]
where the time goes in v1:
time: 284 us
  Pallas kernels  280 us (99%)
  local copies, waits for them, and re-layouts  3.91 us (1%)
    pallas_call x1, Pallas kernels, per_device(): pl.pallas_call(functools.partial(layer_kernel, nfs, ntp, ny, names), out_...  280 us

profile of v1, /device:TPU:0, one launch (start us, length us, event | category | flops | bytes accessed | tf_op | source)
XLA Modules:
  0.0 283.6 jit_solution(18281213515697913760)
XLA Ops:
  0.0 0.0 copy-start
  0.0 0.0 copy-start.1
  0.0 0.7 copy-done
  0.7 0.6 broadcast_in_dim.43.refs_15_
  1.3 0.0 copy-done.1
  1.3 0.6 broadcast_in_dim.44.refs_16_
  1.8 279.7 %layer.1 = bf16[768,512]{1,0:T(8,128)(2,1)} custom-call(f32[256,768]{1,0:T(8,128)} %refs_0_.1, f32[256,768]{1,0:T(8,128)} %refs_1_.1, f32[768,256]{1,0:T(8,128)} %refs_2_.1, f32[256,512]{1,0:T(8,128)} %refs_3_.1, f32[256,512]{1,0:T(8,128)} %refs_4_.1, f32[256,512]{1,0:T(8,128)} %refs_5_.1, f32[256,512]{1,0:T(8,128)} %refs_6_.1, f32[512,256]{1,0:T(8,128)} %refs_7_.1, ...), custom_call_target="tpu_custom_call" | custom-call | flops 40000000000 | bytes 16777216 | tf_op jit(solution)/shard_map/layer/pallas_call | solution.py:598
  281.6 2.1 copy.26
Async XLA Ops:
  0.0 0.7 copy-start
  0.0 1.3 copy-start.1

commit v2 on v1

--- a/solution.py
+++ b/solution.py
@@ -15,10 +15,9 @@
 MESH = pl.DeviceIdType.MESH
 BF16 = jnp.bfloat16
 F32 = jnp.float32
-WEIGHTS = ("gate", "up", "down", "query", "key", "value", "outgate", "mix")
-DIMS = (0, 0, 1, 0, 0, 0, 0, 1)
-PARTS = (2, 2, 2, 1, 1, 1, 1, 2)
-ALONG_Z = ((0, 0), (3, 0))
+WEIGHTS = ("gate", "up", "down", "mix", "query", "key", "value", "outgate")
+DIMS = (0, 0, 1, 1, 0, 0, 0, 0)
+STAGES = (0, 1, 2, 2, 0, 1, 0, 1)
 
 
 def cols_at(index, width):
@@ -58,11 +57,11 @@
 
 
 class TpGather:
-    def __init__(self, group, src, out, sems, rows):
+    def __init__(self, group, out, sems, rows):
         self.group = group
-        self.src, self.out, self.rows = src, out, rows
+        self.out, self.rows = out, rows
         self.sends, self.forwards, self.recvs = sems
-        self.width = src.shape[1]
+        self.width = out.shape[1] // group.ntp
 
     def at(self, piece):
         return pl.ds(piece * self.rows, self.rows)
@@ -77,7 +76,7 @@
             target = group.along_x(offset, group.core) if offset else group.partner
             copies.append(
                 remote(
-                    self.src.at[self.at(piece)], self.place(group.t, piece),
+                    self.place(group.t, piece), self.place(group.t, piece),
                     self.sends.at[offset, piece], self.recvs.at[group.t, piece], "tp", target,
                 )
             )
@@ -113,12 +112,12 @@
         group = self.group
         for offset in range(group.nx):
             self.arrived(group.along_x(offset, 1 - group.core), piece)
-        for offset in range(1, group.nx):
-            self.forward(offset, piece).wait_send()
 
     def finish(self, piece):
         for copy in self.own_sends(piece):
             copy.wait_send()
+        for offset in range(1, self.group.nx):
+            self.forward(offset, piece).wait_send()
 
 
 class TpReduce:
@@ -247,29 +246,26 @@
                         self.move_y(p, index, act)
 
     def schedule(self):
-        count = len(self.pieces)
-        events = [(-1, functools.partial(self.own, 0))]
-        for tick in range(count + self.nz - 2):
-            if tick + 1 < count:
-                events.append((tick, functools.partial(self.own, tick + 1)))
-            if tick < count and self.whole_z(tick):
-                events.append((tick, functools.partial(self.side, tick)))
+        events = []
+        for p in range(len(self.pieces)):
+            late = self.whole_z(p)
+            events.append((p - 1.3 + 0.5 * late, p, functools.partial(self.own, p)))
+            if late:
+                events.append((p + 1.2, p, functools.partial(self.side, p)))
             for distance in range(1, self.nz):
-                if 0 <= tick + 1 - distance < count:
-                    events.append((tick, functools.partial(self.relay, distance, tick + 1 - distance)))
-        return events
+                when = p + 0.75 * distance + (1.55 if late else -0.4)
+                events.append((when, p, functools.partial(self.relay, distance, p)))
+        events.sort(key=lambda event: event[:2])
+        return [event[1:] for event in events]
 
     def some(self, count):
         for _, event in self.events[self.done : self.done + count]:
             event(lambda copy: copy.start(), True)
         self.done = min(self.done + count, len(self.events))
 
-    def upto(self, tick):
-        ahead = sum(1 for at, _ in self.events[self.done :] if at <= tick)
-        self.some(ahead)
-
     def need(self, p):
-        self.upto(p + self.nz - 2)
+        last = max(i for i, (piece, _) in enumerate(self.events) if piece == p)
+        self.some(max(0, last + 1 - self.done))
         if not self.whole_z(p):
             for zs in range(self.nz):
                 for index in self.others(zs):
@@ -298,80 +294,106 @@
 
 def layer_kernel(nfs, ntp, ny, names, *refs):
     r = SimpleNamespace(**dict(zip(names, refs)))
-    rows, width = r.tok.shape
+    rows, width = r.out.shape
+    model = width * ntp
+    half = model // 2
     count = rows // LEN
     chunks = range(count)
     group = TpGroup(ntp)
     shards = [getattr(r, "w_" + name) for name in WEIGHTS]
     wholes = [getattr(r, name) for name in WEIGHTS]
-    pieces, first_of = [], {}
+    pieces, held = [], {name: [] for name in WEIGHTS}
     for i, name in enumerate(WEIGHTS):
-        first_of[name] = len(pieces)
-        size = shards[i].shape[0] // PARTS[i]
-        for part in range(PARTS[i]):
+        height, cols = shards[i].shape
+        along_z = max(16, height * 3 // 16 // 16 * 16)
+        for late, start, size in ((True, 0, along_z), (False, along_z, height - along_z)):
+            held[name].append(len(pieces))
             pieces.append(
                 SimpleNamespace(
-                    buf=wholes[i], dim=DIMS[i], rows=shards[i].shape[0], cols=shards[i].shape[1],
-                    start=part * size, size=size, along_z=(i, part) in ALONG_Z,
+                    buf=wholes[i], dim=DIMS[i], rows=height, cols=cols,
+                    start=start, size=size, along_z=late,
                 )
             )
     stream = FsStream(nfs, ny, pieces, r.w_send, r.w_recv)
 
     def need(name):
-        i = WEIGHTS.index(name)
-        for part in range(PARTS[i]):
-            stream.need(first_of[name] + part)
+        for p in held[name]:
+            stream.need(p)
 
     def at(c):
         return pl.ds(c * LEN, LEN)
 
+    own = cols_at(group.t, width)
+    mine = cols_at(group.core, half)
+    stages = [r.stage_0, r.stage_1, r.stage_2]
+
+    def load(i):
+        height, cols = shards[i].shape
+        stage = stages[STAGES[i]].at[pl.ds(0, height), pl.ds(0, cols)]
+        return pltpu.make_async_copy(shards[i], stage, r.load_sem.at[i])
+
+    def cast(i):
+        load(i).wait()
+        height, cols = shards[i].shape
+        value = stages[STAGES[i]][0:height, 0:cols].astype(BF16)
+        if DIMS[i] == 0:
+            wholes[i][pl.ds(pl.multiple_of(stream.f * height, height), height), :] = value
+        else:
+            wholes[i][:, cols_at(stream.f, cols)] = value
+
     barrier = pltpu.get_barrier_semaphore()
     greeted = group.greet(barrier) + stream.greet(barrier)
-    loads = [
-        pltpu.make_async_copy(shards[i], getattr(r, "stage_" + name), r.load_sem.at[i])
-        for i, name in enumerate(WEIGHTS)
+    tok_load = pltpu.make_async_copy(r.tok, r.full_0.at[:, own], r.tok_sem)
+    table_loads = [
+        pltpu.make_async_copy(src, dst, r.table_sem.at[i])
+        for i, (src, dst) in enumerate(((r.cosines, r.cos), (r.sines, r.sin)))
     ]
-    for load in loads:
-        load.start()
-
-    def cast(i):
-        loads[i].wait()
-        shard = shards[i].shape
-        value = getattr(r, "stage_" + WEIGHTS[i])[...].astype(BF16)
-        if DIMS[i] == 0:
-            wholes[i][pl.ds(pl.multiple_of(stream.f * shard[0], shard[0]), shard[0]), :] = value
-        else:
-            wholes[i][:, cols_at(stream.f, shard[1])] = value
-
+    load(0).start()
+    tok_load.start()
+    load(1).start()
+    load(2).start()
+    for table in table_loads:
+        table.start()
     r.gain_own[...] = jnp.zeros(r.gain_own.shape, F32)
-    for row, ref in enumerate((r.gain_one, r.gain_mix, r.gain_two)):
+    for row, ref in enumerate((r.gain_one, r.gain_mix, r.gain_two, r.scale_mix)):
         r.gain_own[row : row + 1, :] = ref[...]
+    r.gains[:, own] = r.gain_own[...]
+    for src, dst in ((r.scale_gate, r.s_gate), (r.scale_up, r.s_up)):
+        for row in range(src.shape[0]):
+            dst[:, row * 128 : (row + 1) * 128] = src[row : row + 1, :]
     cast(0)
-    cast(1)
-    r.full_0[:, cols_at(group.t, width)] = r.tok[...]
-    r.gains[:, cols_at(group.t, width)] = r.gain_own[...]
     pl.semaphore_wait(barrier, greeted)
 
-    gain_gather = TpGather(group, r.gain_own, r.gains, (r.n_send, r.n_fwd, r.n_recv), 8)
+    gain_gather = TpGather(group, r.gains, (r.n_send, r.n_fwd, r.n_recv), 8)
     gathers = [
-        TpGather(group, src, full, (r.g_send.at[i], r.g_fwd.at[i], r.g_recv.at[i]), LEN)
-        for i, (src, full) in enumerate(
-            ((r.tok, r.full_0), (r.first, r.full_1), (r.second, r.full_2))
-        )
+        TpGather(group, full, (r.g_send.at[i], r.g_fwd.at[i], r.g_recv.at[i]), LEN)
+        for i, full in enumerate((r.full_0, r.full_1, r.mixed))
     ]
     reduces = [
         TpReduce(
             group, r.part, r.pair, r.one.at[i], r.two.at[i],
             (r.r_s1.at[i], r.r_v1.at[i], r.r_s2.at[i], r.r_v2.at[i]), LEN, width,
         )
-        for i in range(3)
+        for i in range(2)
     ]
+    stream.some(2)
     gain_gather.start(0)
+    tok_load.wait()
     for c in chunks:
         gathers[0].start(c)
+    cast(1)
+    load(4).start()
+    load(5).start()
+    cast(2)
+    load(3).start()
     stream.some(2)
-    for i in range(2, len(WEIGHTS)):
-        cast(i)
+    cast(3)
+    cast(4)
+    load(6).start()
+    cast(5)
+    load(7).start()
+    cast(6)
+    cast(7)
 
     def norm(full, row, c):
         gain = r.gains[row : row + 1, :]
@@ -381,86 +403,122 @@
             some = pl.ds(pl.multiple_of(c * LEN + i * step, step), step)
             v = full[some, :].astype(F32)
             mean = jnp.mean(v * v, axis=1, keepdims=True)
-            full[some, :] = (v * lax.rsqrt(mean + EPS) * gain).astype(BF16)
+            r.normed[some, :] = (v * lax.rsqrt(mean + EPS) * gain).astype(BF16)
             return carry
 
         lax.fori_loop(0, LEN // step, body, 0)
 
-    def gate_up(full, c):
+    def gate_up(c):
         units = r.gate.shape[1]
         tile = 256 if units % 256 == 0 else 128
 
         def body(n, carry):
             cols = cols_at(n, tile)
-            x = full[at(c), :]
-            g = dot(x, r.gate[:, cols]) * r.scale_gate[:, cols]
-            u = dot(x, r.up[:, cols]) * r.scale_up[:, cols]
+            x = r.normed[at(c), :]
+            g = dot(x, r.gate[:, cols]) * r.s_gate[:, cols]
+            u = dot(x, r.up[:, cols]) * r.s_up[:, cols]
             r.hidden[at(c), cols] = (g / (1.0 + jnp.exp(-g)) * u).astype(BF16)
             return carry
 
         lax.fori_loop(0, units // tile, body, 0)
 
-    def partial(left, weight, c):
+    def partial(c):
         def body(n, carry):
             cols = cols_at(n, width)
-            r.part[at(c), cols] = dot(left[at(c), :], weight[:, cols]).astype(BF16)
+            r.part[at(c), cols] = dot(r.hidden[at(c), :], r.down[:, cols]).astype(BF16)
             return carry
 
         lax.fori_loop(0, ntp, body, 0)
 
-    def project(name, full):
+    def project(name):
         weight, scale, out = getattr(r, name), getattr(r, "scale_" + name), getattr(r, "a_" + name)
 
         def body(c, carry):
             some = pl.ds(pl.multiple_of(c * LEN, LEN), LEN)
-            out[some, :] = (dot(full[some, :], weight[...]) * scale[...]).astype(BF16)
+            out[some, :] = (dot(r.normed[some, :], weight[...]) * scale[...]).astype(BF16)
             return carry
 
         lax.fori_loop(0, count, body, 0)
 
-    def retain():
-        heads = r.rate.shape[1]
-        size = width // heads
+    heads = r.rate.shape[1]
+    size = width // heads
+
+    def retain(c):
         even = lax.rem(lax.broadcasted_iota(jnp.int32, (LEN, size), 1), 2) == 0
         distance = lax.broadcasted_iota(jnp.int32, (LEN, LEN), 0) - lax.broadcasted_iota(
             jnp.int32, (LEN, LEN), 1
         )
 
-        def body(i, carry):
-            c, h = lax.div(i, heads), lax.rem(i, heads)
-            some, cols = pl.ds(pl.multiple_of(c * LEN, LEN), LEN), cols_at(h, size)
+        def body(h, carry):
+            cols = cols_at(h, size)
 
             def turned(ref):
-                v = ref[some, cols].astype(F32)
+                v = ref[at(c), cols].astype(F32)
                 swapped = jnp.where(even, -pltpu.roll(v, size - 1, 1), pltpu.roll(v, 1, 1))
-                return v * r.cosines[...] + swapped * r.sines[...]
+                return v * r.cos[...] + swapped * r.sin[...]
 
             q = turned(r.a_query).astype(BF16)
             k = (turned(r.a_key) * size ** -0.5).astype(BF16)
             scores = lax.dot_general(q, k, (((1,), (1,)), ((), ())), preferred_element_type=F32)
             decay = jnp.exp(-r.rate[0, h] * jnp.maximum(distance, 0).astype(F32))
             scores = jnp.where(distance >= 0, scores * decay, 0.0).astype(BF16)
-            kept = dot(scores, r.a_value[some, cols])
+            kept = dot(scores, r.a_value[at(c), cols])
             kept = kept * lax.rsqrt(jnp.mean(kept * kept, axis=1, keepdims=True) + HEAD_EPS)
-            g = r.a_outgate[some, cols].astype(F32)
-            gated = kept * r.ret_gain[:, cols] * (g / (1.0 + jnp.exp(-g)))
-            r.mixed[some, cols] = gated.astype(BF16)
+            r.kept[at(c), cols] = kept * r.ret_gain[:, cols]
             return carry
 
-        lax.fori_loop(0, count * heads, body, 0)
-
-    def settle(i, c, factor, scale, res, out):
-        value = res[at(c), :].astype(F32) + factor * reduces[i].total(c) * scale[...]
-        value = value.astype(BF16)
-        out[at(c), :] = value
-        if i < 2:
-            full = (r.full_1, r.full_2)[i]
-            full[at(c), cols_at(group.t, width)] = value
-            gathers[i + 1].start(c)
+        lax.fori_loop(0, heads, body, 0)
+
+    def gated(c):
+        g = dot(r.normed[at(c), :], r.outgate[...]) * r.scale_outgate[...]
+        g = g.astype(BF16).astype(F32)
+        r.mixed[at(c), own] = (r.kept[at(c), :] * (g / (1.0 + jnp.exp(-g)))).astype(BF16)
+
+    def spread_mix(offset):
+        target = lax.rem(group.t + offset, ntp)
+        there = cols_at(lax.rem(target, 2), half)
+        place = pl.ds(pl.multiple_of(group.t * width, width), width)
+        return remote(
+            r.mix.at[:, there], r.mix_all.at[place], r.x_send.at[offset], r.x_recv.at[group.t],
+            "tp", target,
+        )
+
+    def mix_arrived(offset):
+        source = lax.rem(group.t + offset, ntp)
+        place = pl.ds(pl.multiple_of(source * width, width), width)
+        remote(
+            r.mix.at[:, mine], r.mix_all.at[place], r.x_send.at[offset], r.x_recv.at[source],
+            "tp", source,
+        ).wait_recv()
+
+    def swap(c):
+        block = r.full_2.at[at(c), mine]
+        return remote(block, block, r.h_send.at[c], r.h_recv.at[c], "tp", group.partner)
+
+    def swapped(c):
+        block = r.full_2.at[at(c), cols_at(1 - group.core, half)]
+        remote(block, block, r.h_send.at[c], r.h_recv.at[c], "tp", group.partner).wait_recv()
+
+    def second(c):
+        tile = 512
+
+        def body(n, carry):
+            cols = cols_at(n, tile)
+            there = pl.ds(pl.multiple_of(group.core * half + n * tile, tile), tile)
+            total = dot(r.mixed[at(c), :], r.mix_all[:, cols]) * r.gains[3:4, there]
+            r.full_2[at(c), there] = (r.full_1[at(c), there].astype(F32) + total).astype(BF16)
+            return carry
+
+        lax.fori_loop(0, half // tile, body, 0)
+
+    def settle(i, c, res, out, place):
+        value = res[at(c), own].astype(F32)
+        value = value + 0.5 * reduces[i].total(c) * r.scale_down[...]
+        out[at(c), place] = value.astype(BF16)
 
     gain_gather.relay(0)
     for c in chunks:
-        stream.upto(c)
+        stream.some(3)
         gathers[0].relay(c)
     gain_gather.complete(0)
     for c in chunks:
@@ -470,19 +528,24 @@
     need("gate")
     need("up")
     for c in chunks:
-        gate_up(r.full_0, c)
+        gate_up(c)
         stream.some(1)
     need("down")
     for c in chunks:
-        partial(r.hidden, r.down, c)
+        partial(c)
         reduces[0].start(c)
         stream.some(1)
     for c in chunks:
         reduces[0].cross(c)
         stream.some(1)
     for c in chunks:
-        settle(0, c, 0.5, r.scale_down, r.tok, r.first)
-        stream.some(1)
+        settle(0, c, r.full_0, r.full_1, own)
+        gathers[1].start(c)
+        stream.some(1)
+    need("mix")
+    for offset in range(1, ntp):
+        spread_mix(offset).start()
+    r.mix_all[pl.ds(pl.multiple_of(group.t * width, width), width), :] = r.mix[:, mine]
     for c in chunks:
         gathers[1].relay(c)
         stream.some(1)
@@ -490,38 +553,46 @@
         gathers[1].complete(c)
         norm(r.full_1, 1, c)
         reduces[0].finish(c)
-    for name in ("query", "key", "value", "outgate"):
+        stream.some(1)
+    for table in table_loads:
+        table.wait()
+    for name in ("query", "key", "value"):
         need(name)
-        project(name, r.full_1)
-        stream.some(1)
-    retain()
-    need("mix")
-    for c in chunks:
-        partial(r.mixed, r.mix, c)
-        reduces[1].start(c)
-    for c in chunks:
-        reduces[1].cross(c)
-    for c in chunks:
-        settle(1, c, 1.0, r.scale_mix, r.first, r.second)
+        project(name)
+        stream.some(1)
+    for c in chunks:
+        retain(c)
+        stream.some(1)
+    for offset in range(1, ntp):
+        mix_arrived(offset)
+    need("outgate")
+    for c in chunks:
+        gated(c)
+        gathers[2].start(c)
     gathers[2].relay(0)
     for c in chunks:
         gathers[2].complete(c)
-        norm(r.full_2, 2, c)
+        second(c)
+        swap(c).start()
         if c > 0:
-            reduces[2].cross(c - 1)
-        gate_up(r.full_2, c)
+            reduces[1].cross(c - 1)
         if c + 1 < count:
             gathers[2].relay(c + 1)
+        swapped(c)
+        norm(r.full_2, 2, c)
+        gate_up(c)
+        partial(c)
+        reduces[1].start(c)
+    reduces[1].cross(count - 1)
+    for c in chunks:
+        settle(1, c, r.full_2, r.out, pl.ds(0, width))
+    for c in chunks:
         reduces[1].finish(c)
-        partial(r.hidden, r.down, c)
-        reduces[2].start(c)
-    reduces[2].cross(count - 1)
-    for c in chunks:
-        settle(2, c, 0.5, r.scale_down, r.second, r.out)
-    for c in chunks:
-        reduces[2].finish(c)
+        swap(c).wait_send()
         for gather in gathers:
             gather.finish(c)
+    for offset in range(1, ntp):
+        spread_mix(offset).wait_send()
     gain_gather.finish(0)
     stream.finish()
 
@@ -555,45 +626,56 @@
     rows, width = tokens.shape
     count = rows // LEN
     model = width * ntp
-    weights = (w_gate, w_up, w_down, w_query, w_key, w_value, w_outgate, w_mix)
+    weights = (w_gate, w_up, w_down, w_mix, w_query, w_key, w_value, w_outgate)
     cosines, sines = tables(LEN, width // decay_rate.shape[0])
     anywhere = pl.BlockSpec(memory_space=pl.ANY)
     inputs = {"w_" + name: (w, anywhere) for name, w in zip(WEIGHTS, weights)}
-    inputs["tok"] = (tokens, vmem())
+    inputs["tok"] = (tokens, anywhere)
     inputs["rate"] = (decay_rate[None], pl.BlockSpec(memory_space=pltpu.SMEM))
-    inputs["cosines"], inputs["sines"] = (cosines, vmem()), (sines, vmem())
+    inputs["cosines"], inputs["sines"] = (cosines, anywhere), (sines, anywhere)
+    inputs["scale_gate"] = (scale_gate.reshape(-1, 128), vmem())
+    inputs["scale_up"] = (scale_up.reshape(-1, 128), vmem())
     for name, value in (
         ("gain_one", gain_one), ("gain_mix", gain_mix), ("gain_two", gain_two),
-        ("scale_gate", scale_gate), ("scale_up", scale_up), ("scale_down", scale_down),
-        ("scale_query", scale_query), ("scale_key", scale_key), ("scale_value", scale_value),
-        ("scale_outgate", scale_outgate), ("scale_mix", scale_mix), ("ret_gain", ret_gain),
+        ("scale_down", scale_down), ("scale_query", scale_query), ("scale_key", scale_key),
+        ("scale_value", scale_value), ("scale_outgate", scale_outgate),
+        ("scale_mix", scale_mix), ("ret_gain", ret_gain),
     ):
         inputs[name] = (value[None], vmem())
     scratch = {}
     for name, w, dim in zip(WEIGHTS, weights, DIMS):
         grown = tuple(size * (nfs if axis == dim else 1) for axis, size in enumerate(w.shape))
         scratch[name] = pltpu.VMEM(grown, BF16)
-        scratch["stage_" + name] = pltpu.VMEM(w.shape, F32)
     for i in range(3):
-        scratch["full_%d" % i] = pltpu.VMEM((rows, model), BF16)
-    scratch["part"] = pltpu.VMEM((rows, model), BF16)
+        shapes = [w.shape for w, stage in zip(weights, STAGES) if stage == i]
+        scratch["stage_%d" % i] = pltpu.VMEM(tuple(max(sizes) for sizes in zip(*shapes)), F32)
+    for name in ("full_0", "full_1", "full_2", "normed", "mixed", "part"):
+        scratch[name] = pltpu.VMEM((rows, model), BF16)
+    scratch["mix_all"] = pltpu.VMEM((model, model // 2), BF16)
     scratch["hidden"] = pltpu.VMEM((rows, w_gate.shape[1]), BF16)
     far = max(nx - 1, 1)
     scratch["pair"] = pltpu.VMEM((far, rows, width), BF16)
-    scratch["one"] = pltpu.VMEM((3, nx, rows, width), BF16)
-    scratch["two"] = pltpu.VMEM((3, far, rows, width), BF16)
-    for name in ("a_query", "a_key", "a_value", "a_outgate", "mixed", "first", "second"):
+    scratch["one"] = pltpu.VMEM((2, nx, rows, width), BF16)
+    scratch["two"] = pltpu.VMEM((2, far, rows, width), BF16)
+    for name in ("a_query", "a_key", "a_value"):
         scratch[name] = pltpu.VMEM((rows, width), BF16)
+    scratch["kept"] = pltpu.VMEM((rows, width), F32)
+    scratch["cos"], scratch["sin"] = pltpu.VMEM(cosines.shape, F32), pltpu.VMEM(sines.shape, F32)
+    scratch["s_gate"] = pltpu.VMEM((1, w_gate.shape[1]), F32)
+    scratch["s_up"] = pltpu.VMEM((1, w_up.shape[1]), F32)
     scratch["gain_own"] = pltpu.VMEM((8, width), F32)
     scratch["gains"] = pltpu.VMEM((8, model), F32)
-    total = sum(PARTS)
-    scratch["load_sem"] = dma(len(WEIGHTS))
+    total = 2 * len(WEIGHTS)
+    scratch["load_sem"], scratch["tok_sem"] = dma(len(WEIGHTS)), dma()
+    scratch["table_sem"] = dma(2)
     scratch["w_send"], scratch["w_recv"] = dma(ny + 1, nfs, total), dma(nfs, total)
     scratch["n_send"], scratch["n_fwd"], scratch["n_recv"] = dma(nx, 1), dma(nx, 1), dma(ntp, 1)
     scratch["g_send"], scratch["g_fwd"] = dma(3, nx, count), dma(3, nx, count)
     scratch["g_recv"] = dma(3, ntp, count)
-    scratch["r_s1"], scratch["r_v1"] = dma(3, nx, count), dma(3, nx, count)
-    scratch["r_s2"], scratch["r_v2"] = dma(3, far, count), dma(3, far, count)
+    scratch["r_s1"], scratch["r_v1"] = dma(2, nx, count), dma(2, nx, count)
+    scratch["r_s2"], scratch["r_v2"] = dma(2, far, count), dma(2, far, count)
+    scratch["x_send"], scratch["x_recv"] = dma(ntp), dma(ntp)
+    scratch["h_send"], scratch["h_recv"] = dma(count), dma(count)
     names = list(inputs) + ["out"] + list(scratch)
     return pl.pallas_call(
         functools.partial(layer_kernel, nfs, ntp, ny, names),

time: 284 us -> 265 us (0.933)
  Pallas kernels: 280 us -> 263 us
    pallas_call x1, Pallas kernels: 280 us -> 263 us  [per_device(): pl.pallas_call(functools.partial(layer_kernel, nfs, ntp, ny, names), out_...]
where the time goes in v2:
time: 265 us
  Pallas kernels  263 us (99%)
    pallas_call x1, Pallas kernels, per_device(): pl.pallas_call(functools.partial(layer_kernel, nfs, ntp, ny, names), out_...  263 us

profile of v2, /device:TPU:0, one launch (start us, length us, event | category | flops | bytes accessed | tf_op | source)
XLA Modules:
  0.0 264.9 jit_solution(17721959643586051404)
XLA Ops:
  0.0 262.8 %layer.1 = bf16[768,512]{1,0:T(8,128)(2,1)} custom-call(f32[256,768]{1,0:T(8,128)} %refs_0_.1, f32[256,768]{1,0:T(8,128)} %refs_1_.1, f32[768,256]{1,0:T(8,128)} %refs_2_.1, f32[512,256]{1,0:T(8,128)} %refs_3_.1, f32[256,512]{1,0:T(8,128)} %refs_4_.1, f32[256,512]{1,0:T(8,128)} %refs_5_.1, f32[256,512]{1,0:T(8,128)} %refs_6_.1, f32[256,512]{1,0:T(8,128)} %refs_7_.1, ...), custom_call_target="tpu_custom_call" | custom-call | flops 40000000000 | bytes 16777216 | tf_op jit(solution)/shard_map/layer/pallas_call | solution.py:680
  262.8 2.1 copy.26

commit v3 on v2

--- a/solution.py
+++ b/solution.py
@@ -406,21 +406,13 @@
             r.normed[some, :] = (v * lax.rsqrt(mean + EPS) * gain).astype(BF16)
             return carry
 
-        lax.fori_loop(0, LEN // step, body, 0)
+        lax.fori_loop(0, LEN // step, body, 0, unroll=4)
 
     def gate_up(c):
-        units = r.gate.shape[1]
-        tile = 256 if units % 256 == 0 else 128
-
-        def body(n, carry):
-            cols = cols_at(n, tile)
-            x = r.normed[at(c), :]
-            g = dot(x, r.gate[:, cols]) * r.s_gate[:, cols]
-            u = dot(x, r.up[:, cols]) * r.s_up[:, cols]
-            r.hidden[at(c), cols] = (g / (1.0 + jnp.exp(-g)) * u).astype(BF16)
-            return carry
-
-        lax.fori_loop(0, units // tile, body, 0)
+        x = r.normed[at(c), :]
+        g = dot(x, r.gate[...]) * r.s_gate[...]
+        u = dot(x, r.up[...]) * r.s_up[...]
+        r.hidden[at(c), :] = (g / (1.0 + jnp.exp(-g)) * u).astype(BF16)
 
     def partial(c):
         def body(n, carry):
@@ -537,18 +529,18 @@
         stream.some(1)
     for c in chunks:
         reduces[0].cross(c)
-        stream.some(1)
+        stream.some(2)
     for c in chunks:
         settle(0, c, r.full_0, r.full_1, own)
         gathers[1].start(c)
-        stream.some(1)
+        stream.some(2)
     need("mix")
     for offset in range(1, ntp):
         spread_mix(offset).start()
     r.mix_all[pl.ds(pl.multiple_of(group.t * width, width), width), :] = r.mix[:, mine]
     for c in chunks:
         gathers[1].relay(c)
-        stream.some(1)
+        stream.some(2)
     for c in chunks:
         gathers[1].complete(c)
         norm(r.full_1, 1, c)
@@ -563,26 +555,32 @@
     for c in chunks:
         retain(c)
         stream.some(1)
+    need("outgate")
+    for c in chunks:
+        gated(c)
+        gathers[2].start(c)
     for offset in range(1, ntp):
         mix_arrived(offset)
-    need("outgate")
-    for c in chunks:
-        gated(c)
-        gathers[2].start(c)
     gathers[2].relay(0)
-    for c in chunks:
-        gathers[2].complete(c)
-        second(c)
-        swap(c).start()
+    gathers[2].complete(0)
+    second(0)
+    swap(0).start()
+    for c in chunks:
+        swapped(c)
+        norm(r.full_2, 2, c)
+        if c == 0 and count > 1:
+            gathers[2].relay(1)
         if c > 0:
             reduces[1].cross(c - 1)
+        gate_up(c)
         if c + 1 < count:
-            gathers[2].relay(c + 1)
-        swapped(c)
-        norm(r.full_2, 2, c)
-        gate_up(c)
+            gathers[2].complete(c + 1)
+            second(c + 1)
+            swap(c + 1).start()
         partial(c)
         reduces[1].start(c)
+        if c + 2 < count:
+            gathers[2].relay(c + 2)
     reduces[1].cross(count - 1)
     for c in chunks:
         settle(1, c, r.full_2, r.out, pl.ds(0, width))

time: 265 us -> 248 us (0.936)
  Pallas kernels: 263 us -> 246 us
    pallas_call x1, Pallas kernels: 263 us -> 246 us  [per_device(): pl.pallas_call(functools.partial(layer_kernel, nfs, ntp, ny, names), out_...]
where the time goes in v3:
time: 248 us
  Pallas kernels  246 us (99%)
    pallas_call x1, Pallas kernels, per_device(): pl.pallas_call(functools.partial(layer_kernel, nfs, ntp, ny, names), out_...  246 us

profile of v3, /device:TPU:0, one launch (start us, length us, event | category | flops | bytes accessed | tf_op | source)
XLA Modules:
  0.0 247.7 jit_solution(3455501933506710466)
XLA Ops:
  0.0 245.6 %layer.1 = bf16[768,512]{1,0:T(8,128)(2,1)} custom-call(f32[256,768]{1,0:T(8,128)} %refs_0_.1, f32[256,768]{1,0:T(8,128)} %refs_1_.1, f32[768,256]{1,0:T(8,128)} %refs_2_.1, f32[512,256]{1,0:T(8,128)} %refs_3_.1, f32[256,512]{1,0:T(8,128)} %refs_4_.1, f32[256,512]{1,0:T(8,128)} %refs_5_.1, f32[256,512]{1,0:T(8,128)} %refs_6_.1, f32[256,512]{1,0:T(8,128)} %refs_7_.1, ...), custom_call_target="tpu_custom_call" | custom-call | flops 40000000000 | bytes 16777216 | tf_op jit(solution)/shard_map/layer/pallas_call | solution.py:678
  245.6 2.1 copy.26

commit v4 on v3

--- a/solution.py
+++ b/solution.py
@@ -416,11 +416,11 @@
 
     def partial(c):
         def body(n, carry):
-            cols = cols_at(n, width)
+            cols = cols_at(n, half)
             r.part[at(c), cols] = dot(r.hidden[at(c), :], r.down[:, cols]).astype(BF16)
             return carry
 
-        lax.fori_loop(0, ntp, body, 0)
+        lax.fori_loop(0, 2, body, 0)
 
     def project(name):
         weight, scale, out = getattr(r, name), getattr(r, "scale_" + name), getattr(r, "a_" + name)
@@ -492,16 +492,8 @@
         remote(block, block, r.h_send.at[c], r.h_recv.at[c], "tp", group.partner).wait_recv()
 
     def second(c):
-        tile = 512
-
-        def body(n, carry):
-            cols = cols_at(n, tile)
-            there = pl.ds(pl.multiple_of(group.core * half + n * tile, tile), tile)
-            total = dot(r.mixed[at(c), :], r.mix_all[:, cols]) * r.gains[3:4, there]
-            r.full_2[at(c), there] = (r.full_1[at(c), there].astype(F32) + total).astype(BF16)
-            return carry
-
-        lax.fori_loop(0, half // tile, body, 0)
+        total = dot(r.mixed[at(c), :], r.mix_all[...]) * r.gains[3:4, mine]
+        r.full_2[at(c), mine] = (r.full_1[at(c), mine].astype(F32) + total).astype(BF16)
 
     def settle(i, c, res, out, place):
         value = res[at(c), own].astype(F32)

time: 248 us -> 247 us (level)
  no operation moved by 1% of the time
where the time goes in v4:
time: 247 us
  Pallas kernels  245 us (99%)
    pallas_call x1, Pallas kernels, per_device(): pl.pallas_call(functools.partial(layer_kernel, nfs, ntp, ny, names), out_...  245 us

profile of v4, /device:TPU:0, one launch (start us, length us, event | category | flops | bytes accessed | tf_op | source)
XLA Modules:
  0.0 247.0 jit_solution(9888414339717362250)
XLA Ops:
  0.0 245.0 %layer.1 = bf16[768,512]{1,0:T(8,128)(2,1)} custom-call(f32[256,768]{1,0:T(8,128)} %refs_0_.1, f32[256,768]{1,0:T(8,128)} %refs_1_.1, f32[768,256]{1,0:T(8,128)} %refs_2_.1, f32[512,256]{1,0:T(8,128)} %refs_3_.1, f32[256,512]{1,0:T(8,128)} %refs_4_.1, f32[256,512]{1,0:T(8,128)} %refs_5_.1, f32[256,512]{1,0:T(8,128)} %refs_6_.1, f32[256,512]{1,0:T(8,128)} %refs_7_.1, ...), custom_call_target="tpu_custom_call" | custom-call | flops 40000000000 | bytes 16777216 | tf_op jit(solution)/shard_map/layer/pallas_call | solution.py:670
  245.0 2.1 copy.26
